TPU v7x, 32 devices: a whole 2x2x4 slice. The times are simulated.
32 devices in a mesh: grp: 2 (over y), fs: 4 (over z), tp: 4 (over x, core).
Axes of the slice: x: 2, y: 2, z: 4, core: 2. Of those that a mesh axis runs over, the one named last changes fastest.
Arguments:
- hidden_activations: bfloat16 [2048, 6144], P('tp', ('grp', 'fs')), parts along dimension 1, may hold values from -6 to 6
- attention_rescaling_factors: float32 [2048], replicated, may hold values from 0.1 to 1.9
- feature_rescaling_factors: float32 [2048], replicated, may hold values from 0.1 to 1.9
- request_matrix: float32 [2048, 2048], P('fs', 'tp'), may hold values from -0.125 to 0.125
- request_matrix_multipliers: float32 [2048], P('tp'), may hold values from 0.1 to 1.9
- lookup_matrix: float32 [2048, 2048], P('fs', 'tp'), may hold values from -0.125 to 0.125
- lookup_matrix_multipliers: float32 [2048], P('tp'), may hold values from 0.1 to 1.9
- content_matrix: float32 [2048, 4096], P('fs', 'tp'), may hold values from -0.125 to 0.125
- content_matrix_multipliers: float32 [4096], P('tp'), may hold values from 0.1 to 1.9
- valve_matrix: float32 [2048, 4096], P('fs', 'tp'), may hold values from -0.125 to 0.125
- valve_matrix_multipliers: float32 [4096], P('tp'), may hold values from 0.1 to 1.9
- result_matrix: float32 [4096, 2048], P('tp', 'fs'), may hold values from -0.09375 to 0.09375
- result_matrix_multipliers: float32 [2048], P('fs'), may hold values from 0.1 to 1.9
- expanding_matrix: float32 [2048, 8192], P('fs', 'tp'), may hold values from -0.125 to 0.125
- expand_matrix_multipliers: float32 [8192], P('tp'), may hold values from 0.1 to 1.9
- shrinking_matrix: float32 [8192, 2048], P('tp', 'fs'), may hold values from -0.0625 to 0.0625
- shrink_matrix_multipliers: float32 [2048], P('fs'), may hold values from 0.1 to 1.9
- attention_fading_logarithm: float32 [8], P('tp'), may hold values from -1 to 0
- spike_fading_logarithm: float32 [8, 6144], P('tp', ('grp', 'fs')), parts along dimension 1, may hold values from -1 to 0, as said below
Outputs:
- out_stream: bfloat16 [2048, 6144], P('tp', ('grp', 'fs')), parts along dimension 1
There are 2 independent parts, one for each index of `grp`. A program takes and returns all parts, laid end to end along the dimension named above; an argument that names none is the same for every part. Nothing has to cross between parts.
Inputs may be any that keep to these rules, and one draw needn't show every extreme that they name: `spike_fading_logarithm`: log decay added to the head's own.
All inputs are finite; a program needn't handle non-finite values.
Results may differ from a plain program's by a relative error of at most 0.019.
Values may be sent and summed in bfloat16 or wider, within the bound.
A program may use at most 128 MiB of HBM per device.

v0:
```python
import jax
import jax.numpy as jnp
from jax import lax
from jax.sharding import PartitionSpec as P

DK = 256
DV = 512
BLOCK_POSITIONS = 128
epsilon = 1e-06


def as_sent(value):

    def short(part):
        return part.astype(jnp.bfloat16) if part.dtype == jnp.float32 else part

    return jax.tree.map(short, value)


def rms_norm(matrix, norm_gain):
    values = matrix.astype(jnp.float32)
    factor = lax.rsqrt(jnp.mean(values * values, axis=0, keepdims=True) + epsilon)
    return (values * factor * norm_gain[:, None]).astype(jnp.bfloat16)


def project(normed, weight):
    return lax.dot_general(
        normed, weight, (((0,), (0,)), ((), ())), preferred_element_type=jnp.float32
    )


def collect_features(matrix):
    return lax.all_gather(matrix, "tp", axis=0, tiled=True)


def retain(query, keys, values, fading_logarithm_speed):
    length = query.shape[2]
    causal = jnp.arange(length)[:, None] >= jnp.arange(length)[None, :]

    def advance(memory, inputs):
        query_blk, key_blk, value_blk, rate_blk = inputs
        running = jnp.cumsum(rate_blk, axis=-1)
        closing = running[:, -1:]
        spread = jnp.where(causal, running[:, :, None] - running[:, None, :], 0.0)
        decays = jnp.where(causal, jnp.exp(spread), 0.0)
        scores = (
            jnp.einsum("gid,gjd->gij", query_blk, key_blk, preferred_element_type=jnp.float32)
            * decays
        )
        weights = scores.astype(jnp.bfloat16)
        within = jnp.einsum("gij,gjv->giv", weights, value_blk, preferred_element_type=jnp.float32)
        state_copy = memory.astype(jnp.bfloat16)
        carried = (
            jnp.einsum("gid,gdv->giv", query_blk, state_copy, preferred_element_type=jnp.float32)
            * jnp.exp(running)[:, :, None]
        )
        faded_keys = (key_blk.astype(jnp.float32) * jnp.exp(closing - running)[:, :, None]).astype(
            jnp.bfloat16
        )
        memory = memory * jnp.exp(closing)[:, :, None] + jnp.einsum(
            "gjd,gjv->gdv", faded_keys, value_blk, preferred_element_type=jnp.float32
        )
        return (memory, within + carried)

    initial = jnp.zeros((query.shape[0], query.shape[3], values.shape[3]), jnp.float32)
    stacked = tuple(
        (jnp.swapaxes(member, 0, 1) for member in (query, keys, values, fading_logarithm_speed))
    )
    _, outputs = lax.scan(advance, initial, stacked)
    return jnp.swapaxes(outputs, 0, 1)


def to_heads(matrix, width):
    token_inputs = matrix.shape[0]
    split = matrix.reshape(
        token_inputs // BLOCK_POSITIONS, BLOCK_POSITIONS, matrix.shape[1] // width, width
    )
    return jnp.transpose(split, (2, 0, 1, 3))


def group_norm(retained):
    center = jnp.mean(retained, axis=-1, keepdims=True)
    offset = retained - center
    variance = jnp.mean(offset * offset, axis=-1, keepdims=True)
    return offset * lax.rsqrt(variance + epsilon)


def squared_relu(summed, column_scale):
    rising = jax.nn.relu(summed * column_scale)
    return (rising * rising).astype(jnp.bfloat16)


def local(
    hidden_activations,
    attention_rescaling_factors,
    feature_rescaling_factors,
    request_matrix,
    request_matrix_multipliers,
    lookup_matrix,
    lookup_matrix_multipliers,
    content_matrix,
    content_matrix_multipliers,
    valve_matrix,
    valve_matrix_multipliers,
    result_matrix,
    result_matrix_multipliers,
    expanding_matrix,
    expand_matrix_multipliers,
    shrinking_matrix,
    shrink_matrix_multipliers,
    attention_fading_logarithm,
    spike_fading_logarithm,
):
    out_scales, down_scales = (
        lax.all_gather(result_matrix_multipliers, "fs", axis=0, tiled=True),
        lax.all_gather(shrink_matrix_multipliers, "fs", axis=0, tiled=True),
    )
    normed = rms_norm(collect_features(hidden_activations), attention_rescaling_factors)
    token_inputs = normed.shape[1]
    matrices = (request_matrix, lookup_matrix, content_matrix, valve_matrix)
    pieces = jax.tree.map(
        lambda part: lax.all_gather(part, "fs", axis=0, tiled=True),
        as_sent(tuple((matrix.astype(jnp.bfloat16) for matrix in matrices))),
    )
    picked = normed
    query_sum, key_sum, value_sum, gate_sum = tuple(
        (project(picked, segment) for segment in pieces)
    )
    query = (query_sum * request_matrix_multipliers).astype(jnp.bfloat16)
    keys = (key_sum * lookup_matrix_multipliers * DK ** (-0.5)).astype(jnp.bfloat16)
    values = (value_sum * content_matrix_multipliers).astype(jnp.bfloat16)
    gate = gate_sum * valve_matrix_multipliers
    shard_heads = attention_fading_logarithm.shape[0]
    fading_logarithm_speed = (attention_fading_logarithm[:, None] + spike_fading_logarithm).reshape(
        shard_heads, token_inputs // BLOCK_POSITIONS, BLOCK_POSITIONS
    )
    retained = retain(
        to_heads(query, DK), to_heads(keys, DK), to_heads(values, DV), fading_logarithm_speed
    )
    retained = jnp.transpose(retained, (1, 2, 0, 3)).reshape(token_inputs, shard_heads, DV)
    heads_out = (
        group_norm(retained).reshape(token_inputs, shard_heads * DV) * jax.nn.silu(gate)
    ).astype(jnp.bfloat16)
    out_whole = lax.all_gather(result_matrix.astype(jnp.bfloat16), "fs", axis=1, tiled=True)
    factors = out_scales
    update = lax.psum_scatter(
        (
            lax.dot_general(
                out_whole, heads_out, (((0,), (1,)), ((), ())), preferred_element_type=jnp.float32
            )
            * factors[:, None]
        ).astype(jnp.bfloat16),
        "tp",
        scatter_dimension=0,
        tiled=True,
    ).astype(jnp.float32)
    middle = (hidden_activations.astype(jnp.float32) + update).astype(jnp.bfloat16)
    normed_mlp = rms_norm(collect_features(middle), feature_rescaling_factors)
    picked = normed_mlp
    up_sum = project(
        picked, lax.all_gather(expanding_matrix.astype(jnp.bfloat16), "fs", axis=0, tiled=True)
    )
    hidden = squared_relu(up_sum, expand_matrix_multipliers)
    factors = down_scales
    terms = (
        lax.dot_general(
            lax.all_gather(shrinking_matrix.astype(jnp.bfloat16), "fs", axis=1, tiled=True),
            hidden,
            (((0,), (1,)), ((), ())),
            preferred_element_type=jnp.float32,
        )
        * factors[:, None]
    )
    lowered = lax.psum_scatter(
        terms.astype(jnp.bfloat16), "tp", scatter_dimension=0, tiled=True
    ).astype(jnp.float32)
    return (middle.astype(jnp.float32) + lowered).astype(jnp.bfloat16)


def solution(mesh):
    placed = (
        P("tp", ("grp", "fs")),
        P(),
        P(),
        P("fs", "tp"),
        P("tp"),
        P("fs", "tp"),
        P("tp"),
        P("fs", "tp"),
        P("tp"),
        P("fs", "tp"),
        P("tp"),
        P("tp", "fs"),
        P("fs"),
        P("fs", "tp"),
        P("tp"),
        P("tp", "fs"),
        P("fs"),
        P("tp"),
        P("tp", ("grp", "fs")),
    )
    return jax.shard_map(
        local, mesh=mesh, in_specs=placed, out_specs=P("tp", ("grp", "fs")), check_vma=False
    )
```

profile of v0, /device:TPU:0, one launch (start us, length us, event | category | flops | bytes accessed | tf_op | source)
XLA Modules:
  0.0 824.8 jit_solution(7764887072463206395)
XLA Ops:
  7.3 2.2 convert_element_type.93
  11.8 2.8 convert_element_type.99
  16.1 14.3 %all-gather = f32[4,1,512]{2,1,0:T(1,128)} all-gather(f32[1,1,512]{2,1,0:T(1,128)S(1)} %bitcast.91), channel_id=1, replica_groups=mesh['grp'=2,'fs'=4,'tp'=4] {'fs'}, dimensions={0}, use_global_device_ids=true | all-gather | bytes 10240 | tf_op jit(solution)/shard_map/all_gather | solution.py:115
  30.5 9.7 %all-gather.12.cloned.1.call-done = bf16[2048,768]{1,0:T(8,128)(2,1)} async-done(((bf16[512,768]{1,0:T(8,128)(2,1)}), bf16[2048,768]{1,0:T(8,128)(2,1)}) %all-gather.12.cloned.1.call-update) | async-done | bytes 3145744 | tf_op jit(solution)/shard_map/all_gather | solution.py:33
  40.2 2.6 fusion.39
  42.8 44.7 %all-gather.14.cloned.1.call-done = bf16[2048,512]{1,0:T(8,128)(2,1)} async-done(((bf16[512,512]{1,0:T(8,128)(2,1)}), bf16[2048,512]{1,0:T(8,128)(2,1)}) %all-gather.14.cloned.1.call-update) | async-done | bytes 2097168 | tf_op jit(solution)/shard_map/all_gather | solution.py:122
  87.4 4.5 multiply_convert_fusion.8
  92.1 41.4 %all-gather.18.cloned.1.call-done = bf16[2048,512]{1,0:T(8,128)(2,1)} async-done(((bf16[512,512]{1,0:T(8,128)(2,1)}), bf16[2048,512]{1,0:T(8,128)(2,1)}) %all-gather.18.cloned.1.call-update) | async-done | bytes 2097168 | tf_op jit(solution)/shard_map/all_gather | solution.py:122
  133.5 4.5 multiply_convert_fusion.7
  139.6 74.9 %all-gather.16.cloned.1.call-done = bf16[2048,1024]{1,0:T(8,128)(2,1)} async-done(((bf16[512,1024]{1,0:T(8,128)(2,1)}), bf16[2048,1024]{1,0:T(8,128)(2,1)}) %all-gather.16.cloned.1.call-update) | async-done | bytes 4194320 | tf_op jit(solution)/shard_map/all_gather | solution.py:122
  214.5 6.9 multiply_convert_fusion.6
  221.4 2.6 reshape.102
  225.8 31.8 %while.14 = (s32[]{:T(128)}, f32[2,256,512]{2,1,0:T(8,128)S(1)}, f32[6,2,128,512]{3,2,1,0:T(8,128)}, f32[6,2,128]{2,1,0:T(2,128)S(1)}, bf16[6,2,128,256]{3,2,1,0...) while((s32[]{:T(128)}, f32[2,256,512]{2,1,0:T(8,128)S(1)}, ...), condition=%wide.region_3.4_spmd.clone.clone, body=%wide.region_1.3_spmd.clone.clone.sunk | while | flops 186269696 | bytes 5815448 | solution.py:69
  257.6 2.4 bitcast_reduce_fusion
  262.3 2.4 copy.47
  265.9 2.4 copy.46
  268.4 2.4 copy.40
  270.9 2.4 copy.45
  273.3 21.9 %all-gather.20.cloned.1.call-done = bf16[2048,1024]{1,0:T(8,128)(2,1)} async-done(((bf16[512,1024]{1,0:T(8,128)(2,1)}), bf16[2048,1024]{1,0:T(8,128)(2,1)}) %all-gather.20.cloned.1.call-update) | async-done | bytes 4194320 | tf_op jit(solution)/shard_map/all_gather | solution.py:122
  295.2 80.7 %all-gather.22.cloned.1.call-done = bf16[1024,2048]{1,0:T(8,128)(2,1)} async-done(((bf16[1024,512]{1,0:T(8,128)(2,1)}), bf16[1024,2048]{1,0:T(8,128)(2,1)}) %all-gather.22.cloned.1.call-update) | async-done | bytes 4194320 | tf_op jit(solution)/shard_map/all_gather | solution.py:144
  375.9 15.5 %fusion.49 = bf16[2048,768]{0,1:T(8,128)(2,1)} fusion(f32[2048]{0:T(1024)S(1)} %bitcast.89, bf16[1024,2048]{1,0:T(8,128)(2,1)} %all-gather.22.cloned.1.call-done, f32[768,1024]{1,0:T(8,128)} %bitcast.86, f32[768,1024]{1,0:T(8,128)} %bitcast.88, f32[768,1024]{1,0:T(8,128)} %bitcast.87, bf16[2048,1024]{1,0:T(8,128)(2,1)} %all-gather.20.cloned.1.call-done, ...), kind=kOutput, calls=%fused_computation.63 | convolution fusion | flops 6458966016 | bytes 24140800 | tf_op jit(solution)/shard_map/dot_general | solution.py:148
  392.8 35.0 %reduce-scatter.3.cloned.1.call-done = bf16[512,768]{0,1:T(8,128)(2,1)} async-done(((bf16[2048,768]{0,1:T(8,128)(2,1)}), bf16[512,768]{0,1:T(8,128)(2,1)}) %reduce-scatter.3.cloned.1.call-update) | async-done | bytes 786448 | tf_op jit(solution)/shard_map/reduce_scatter | solution.py:146
  427.7 2.2 add_convert_fusion.1
  430.0 3.9 convert_element_type.109
  434.0 3.9 convert_element_type.111
  437.9 12.2 %all-gather.1 = f32[4,1,512]{2,1,0:T(1,128)S(1)} all-gather(f32[1,1,512]{2,1,0:T(1,128)S(1)} %bitcast.92), channel_id=1, replica_groups=mesh['grp'=2,'fs'=4,'tp'=4] {'fs'}, dimensions={0}, use_global_device_ids=true | all-gather | bytes 10240 | tf_op jit(solution)/shard_map/all_gather | solution.py:116
  450.1 8.6 %all-gather.24.cloned.1.call-done = bf16[2048,768]{0,1:T(8,128)(2,1)} async-done(((bf16[512,768]{0,1:T(8,128)(2,1)}), bf16[2048,768]{0,1:T(8,128)(2,1)}) %all-gather.24.cloned.1.call-update) | async-done | bytes 3145744 | tf_op jit(solution)/shard_map/all_gather | solution.py:33
  458.6 2.7 fusion.42
  461.4 148.5 %all-gather.26.cloned.1.call-done = bf16[2048,2048]{1,0:T(8,128)(2,1)} async-done(((bf16[512,2048]{1,0:T(8,128)(2,1)}), bf16[2048,2048]{1,0:T(8,128)(2,1)}) %all-gather.26.cloned.1.call-update) | async-done | bytes 8388624 | tf_op jit(solution)/shard_map/all_gather | solution.py:161
  609.9 149.2 %all-gather.28.cloned.1.call-done = bf16[2048,2048]{1,0:T(8,128)(2,1)} async-done(((bf16[2048,512]{1,0:T(8,128)(2,1)}), bf16[2048,2048]{1,0:T(8,128)(2,1)}) %all-gather.28.cloned.1.call-update) | async-done | bytes 8388624 | tf_op jit(solution)/shard_map/all_gather | solution.py:167
  759.1 20.6 %fusion.48 = bf16[2048,768]{0,1:T(8,128)(2,1)} fusion(f32[2048]{0:T(1024)S(1)} %bitcast.90, bf16[2048,2048]{1,0:T(8,128)(2,1)} %all-gather.28.cloned.1.call-done, bf16[2048,2048]{1,0:T(8,128)(2,1)} %all-gather.26.cloned.1.call-done, bf16[2048,768]{0,1:T(8,128)(2,1)S(1)} %copy-done.3, f32[2048]{0:T(1024)S(1)} %copy-done.17, f32[2048]{0:T(1024)S(1)} %copy-done.18, ...), kind=kOutput, calls=%fused_computation.62 | convolution fusion | flops 12900630528 | bytes 23096320 | tf_op jit(solution)/shard_map/dot_general | solution.py:166
  779.7 36.1 %reduce-scatter.5.cloned.1.call-done = bf16[512,768]{0,1:T(8,128)(2,1)} async-done(((bf16[2048,768]{0,1:T(8,128)(2,1)}), bf16[512,768]{0,1:T(8,128)(2,1)}) %reduce-scatter.5.cloned.1.call-update) | async-done | bytes 786448 | tf_op jit(solution)/shard_map/reduce_scatter | solution.py:174
  (138 shorter events, 47.3 us)
Async XLA Ops:
  6.5 3.1 copy-start.7
  6.5 4.0 copy-start.5
  6.5 33.6 %all-gather.12.cloned.1.call-start = ((), (), s32[]{:S(2)}) async-start(), calls=%async_computation.2 | async-start | bytes 3932160 | tf_op jit(solution)/shard_map/all_gather | solution.py:33
  7.3 80.2 %all-gather.14.cloned.1.call-start = ((), (), s32[]{:S(2)}) async-start(), calls=%async_computation.3 | async-start | bytes 2621440 | tf_op jit(solution)/shard_map/all_gather | solution.py:122
  9.6 123.9 %all-gather.18.cloned.1.call-start = ((), (), s32[]{:S(2)}) async-start(), calls=%async_computation.5 | async-start | bytes 2621440 | tf_op jit(solution)/shard_map/all_gather | solution.py:122
  10.5 204.0 %all-gather.16.cloned.1.call-start = ((), (), s32[]{:S(2)}) async-start(), calls=%async_computation.4 | async-start | bytes 5242880 | tf_op jit(solution)/shard_map/all_gather | solution.py:122
  11.8 3.0 copy-start.6
  11.8 283.4 %all-gather.20.cloned.1.call-start = ((), (), s32[]{:S(2)}) async-start(), calls=%async_computation.6 | async-start | bytes 5242880 | tf_op jit(solution)/shard_map/all_gather | solution.py:122
  14.7 15.7 %copy-start.9 = (f32[2,768]{1,0:T(2,128)S(1)}, f32[2,768]{1,0:T(2,128)}, u32[]{:S(2)}) copy-start(f32[2,768]{1,0:T(2,128)} %param.39) | copy-start | bytes 18436
  14.7 15.7 %copy-start.14 = (f32[2]{0:T(128)S(1)}, f32[2]{0:T(128)}, u32[]{:S(2)}) copy-start(f32[2]{0:T(128)} %param.38) | copy-start | bytes 28
  14.7 72.7 %copy-start.15 = (f32[2048]{0:T(1024)S(1)}, f32[2048]{0:T(1024)}, u32[]{:S(2)}) copy-start(f32[2048]{0:T(1024)} %param.22) | copy-start | bytes 24580
  14.7 72.7 %copy-start.21 = (f32[512]{0:T(512)S(1)}, f32[512]{0:T(512)}, u32[]{:S(2)}) copy-start(f32[512]{0:T(512)} %param.27) | copy-start | bytes 6148
  14.7 361.1 %all-gather.22.cloned.1.call-start = ((), (), s32[]{:S(2)}) async-start(), calls=%async_computation.7 | async-start | bytes 5242880 | tf_op jit(solution)/shard_map/all_gather | solution.py:144
  16.0 411.7 %reduce-scatter.3.cloned.1.call-start = ((), (), s32[]{:S(2)}) async-start(), calls=%async_computation.8 | async-start | bytes 3932160 | tf_op jit(solution)/shard_map/reduce_scatter | solution.py:146
  42.7 171.8 %copy-start.10 = (f32[768]{0:T(1024)}, f32[768]{0:T(1024)S(1)}, u32[]{:S(2)}) copy-start(f32[768]{0:T(1024)S(1)} %add_rsqrt_fusion.1) | copy-start | bytes 9220
  42.8 90.7 %copy-start.22 = (f32[512]{0:T(512)S(1)}, f32[512]{0:T(512)}, u32[]{:S(2)}) copy-start(f32[512]{0:T(512)} %param.25) | copy-start | bytes 6148
  138.0 76.5 %copy-start.19 = (f32[1024]{0:T(1024)S(1)}, f32[1024]{0:T(1024)}, u32[]{:S(2)}) copy-start(f32[1024]{0:T(1024)} %param.29) | copy-start | bytes 12292
  257.6 2.9 copy-start
  270.8 105.1 %copy-start.2 = (bf16[2048,768]{1,0:T(8,128)(2,1)S(1)}, bf16[2048,768]{1,0:T(8,128)(2,1)}, u32[]{:S(2)}) copy-start(bf16[2048,768]{1,0:T(8,128)(2,1)} %all-gather.12.cloned.1.call-done) | copy-start | bytes 9437188
  270.8 105.0 %copy-start.8 = (f32[4,1,512]{2,1,0:T(1,128)S(1)}, f32[4,1,512]{2,1,0:T(1,128)}, u32[]{:S(2)}) copy-start(f32[4,1,512]{2,1,0:T(1,128)} %all-gather) | copy-start | bytes 24580
  270.8 105.0 %copy-start.11 = (f32[768]{0:T(1024)S(1)}, f32[768]{0:T(1024)}, u32[]{:S(2)}) copy-start(f32[768]{0:T(1024)} %copy-done.10) | copy-start | bytes 9220
  270.8 105.0 %copy-start.16 = (f32[2048]{0:T(1024)S(1)}, f32[2048]{0:T(1024)}, u32[]{:S(2)}) copy-start(f32[2048]{0:T(1024)} %param.22) | copy-start | bytes 24580
  270.9 105.0 %copy-start.20 = (f32[1024]{0:T(1024)S(1)}, f32[1024]{0:T(1024)}, u32[]{:S(2)}) copy-start(f32[1024]{0:T(1024)} %param.31) | copy-start | bytes 12292
  391.4 67.3 %all-gather.24.cloned.1.call-start = ((), (), s32[]{:S(2)}) async-start(), calls=%async_computation.9 | async-start | bytes 3932160 | tf_op jit(solution)/shard_map/all_gather | solution.py:33
  430.0 179.9 %all-gather.26.cloned.1.call-start = ((), (), s32[]{:S(2)}) async-start(), calls=%async_computation.10 | async-start | bytes 10485760 | tf_op jit(solution)/shard_map/all_gather | solution.py:161
  433.9 4.0 copy-start.13
  433.9 325.2 %all-gather.28.cloned.1.call-start = ((), (), s32[]{:S(2)}) async-start(), calls=%async_computation.11 | async-start | bytes 10485760 | tf_op jit(solution)/shard_map/all_gather | solution.py:167
  437.8 321.3 %copy-start.17 = (f32[2048]{0:T(1024)S(1)}, f32[2048]{0:T(1024)}, u32[]{:S(2)}) copy-start(f32[2048]{0:T(1024)} %param.35) | copy-start | bytes 24580
  437.8 321.3 %copy-start.18 = (f32[2048]{0:T(1024)S(1)}, f32[2048]{0:T(1024)}, u32[]{:S(2)}) copy-start(f32[2048]{0:T(1024)} %param.23) | copy-start | bytes 24580
  437.9 377.9 %reduce-scatter.5.cloned.1.call-start = ((), (), s32[]{:S(2)}) async-start(), calls=%async_computation.12 | async-start | bytes 3932160 | tf_op jit(solution)/shard_map/reduce_scatter | solution.py:174
  458.6 300.5 %copy-start.3 = (bf16[2048,768]{0,1:T(8,128)(2,1)S(1)}, bf16[2048,768]{0,1:T(8,128)(2,1)}, u32[]{:S(2)}) copy-start(bf16[2048,768]{0,1:T(8,128)(2,1)} %all-gather.24.cloned.1.call-done) | copy-start | bytes 9437188
  779.7 36.1 %copy-start.1 = (bf16[512,768]{0,1:T(8,128)(2,1)S(1)}, bf16[512,768]{0,1:T(8,128)(2,1)}, u32[]{:S(2)}) copy-start(bf16[512,768]{0,1:T(8,128)(2,1)} %add_convert_fusion.1) | copy-start | bytes 2359300
  (2 other events, 2.6 us)
Sparse Core Ops, SparseCore 0:
  8.9 31.2 all-gather.11
  41.7 45.6 all-gather.13
  89.0 44.4 all-gather.17
  134.9 79.5 all-gather.15
  215.9 79.2 all-gather.19
  296.6 79.2 all-gather.21
  391.5 36.1 reduce-scatter.2
  430.1 28.5 all-gather.23
  460.2 149.6 all-gather.25
  611.3 147.7 all-gather.27
  779.9 35.8 reduce-scatter.4
where the time goes:
time: 826 us; the launch traced here: 825 us
  waiting for transfers between devices  651 us (79%)
  matrix products  79.9 us (10%)
  other arithmetic  30.3 us (4%)
  blocking collectives  26.4 us (3%)
  local copies, waits for them, and re-layouts  22.6 us (3%)
  between operations  13.5 us (2%)
    all_gather x4, waiting for transfers between devices, local(): lax.all_gather(part, 'fs', axis=0, tiled=True)  183 us
    all_gather x1, waiting for transfers between devices, local(): lax.all_gather(shrinking_matrix.astype(jnp.bfloat16), 'fs', axis=1, tiled...  149 us
    all_gather x1, waiting for transfers between devices, local(): lax.all_gather(expanding_matrix.astype(jnp.bfloat16), 'fs', axis=0, tiled...  148 us
    all_gather x1, waiting for transfers between devices, local(): lax.all_gather(result_matrix.astype(jnp.bfloat16), 'fs', axis=1, tiled=True)  80.7 us
    reduce_scatter x1, waiting for transfers between devices, local(): lax.psum_scatter(terms.astype(jnp.bfloat16), 'tp', scatter_dimension=0, t...  36.1 us
    reduce_scatter x1, waiting for transfers between devices, local(): lax.psum_scatter((lax.dot_general(out_whole, heads_out, (((0,), (1,)), ((...  35 us
    dot_general x1, matrix products, local(): lax.dot_general(lax.all_gather(shrinking_matrix.astype(jnp.bfloat16), 'fs...  20.6 us
    all_gather x2, waiting for transfers between devices, collect_features(): return lax.all_gather(matrix, 'tp', axis=0, tiled=True)  18.2 us
  transfers between devices with their start and end apart: 11, of which 11 were waited for; matrix products, arithmetic and copies ran while one was open for 11% of the time, Pallas kernels for 0%

commit v1 on v0

--- a/solution.py
+++ b/solution.py
@@ -141,7 +141,9 @@
     heads_out = (
         group_norm(retained).reshape(token_inputs, shard_heads * DV) * jax.nn.silu(gate)
     ).astype(jnp.bfloat16)
-    out_whole = lax.all_gather(result_matrix.astype(jnp.bfloat16), "fs", axis=1, tiled=True)
+    own = result_matrix.astype(jnp.bfloat16)
+    repeated = jnp.stack([own] * lax.axis_size("fs"))
+    out_whole = jnp.concatenate(lax.all_to_all(repeated, "fs", 0, 0), axis=1)
     factors = out_scales
     update = lax.psum_scatter(
         (

time: 826 us -> 803 us (0.972)
  waiting for transfers between devices: 651 us -> 503 us
  blocking collectives: 26.4 us -> 144 us
    all_gather x1, blocking collectives: 14.3 us -> 132 us  [local(): lax.all_gather(result_matrix_multipliers, 'fs', axis=0, tiled=True)]
    all_gather x1 -> x0, waiting for transfers between devices: 80.7 us -> none  [local(): lax.all_gather(result_matrix.astype(jnp.bfloat16), 'fs', axis=1, tiled=True)]
    all_gather x4, waiting for transfers between devices: 183 us -> 125 us  [local(): lax.all_gather(part, 'fs', axis=0, tiled=True)]
    all_gather x2, waiting for transfers between devices: 18.2 us -> 8.55 us  [collect_features(): return lax.all_gather(matrix, 'tp', axis=0, tiled=True)]
  transfers between devices with their start and end apart: 11 -> 11, of which waited for: 11 -> 8; matrix products, arithmetic and copies ran while one was open for 11% -> 12% of each run, Pallas kernels for 0% -> 0%
where the time goes in v1:
time: 803 us; the launch traced here: 802 us
  waiting for transfers between devices  503 us (63%)
  blocking collectives  144 us (18%)
  matrix products  79.9 us (10%)
  other arithmetic  29.2 us (4%)
  local copies, waits for them, and re-layouts  25.7 us (3%)
  between operations  13.9 us (2%)
    all_gather x1, waiting for transfers between devices, local(): lax.all_gather(shrinking_matrix.astype(jnp.bfloat16), 'fs', axis=1, tiled...  149 us
    all_gather x1, waiting for transfers between devices, local(): lax.all_gather(expanding_matrix.astype(jnp.bfloat16), 'fs', axis=0, tiled...  148 us
    all_gather x1, blocking collectives, local(): lax.all_gather(result_matrix_multipliers, 'fs', axis=0, tiled=True)  132 us
    all_gather x4, waiting for transfers between devices, local(): lax.all_gather(part, 'fs', axis=0, tiled=True)  125 us
    reduce_scatter x1, waiting for transfers between devices, local(): lax.psum_scatter(terms.astype(jnp.bfloat16), 'tp', scatter_dimension=0, t...  36.1 us
    reduce_scatter x1, waiting for transfers between devices, local(): lax.psum_scatter((lax.dot_general(out_whole, heads_out, (((0,), (1,)), ((...  35 us
    dot_general x1, matrix products, local(): lax.dot_general(lax.all_gather(shrinking_matrix.astype(jnp.bfloat16), 'fs...  20.6 us
  transfers between devices with their start and end apart: 11, of which 8 were waited for; matrix products, arithmetic and copies ran while one was open for 12% of the time, Pallas kernels for 0%

profile of v1, /device:TPU:0, one launch (start us, length us, event | category | flops | bytes accessed | tf_op | source)
XLA Modules:
  0.0 802.4 jit_solution(2741615474646970527)
XLA Ops:
  7.3 2.3 convert_element_type.93
  14.1 2.5 stack.2
  16.6 6.6 all-to-all-start
  24.6 131.5 %all-gather = f32[4,1,512]{2,1,0:T(1,128)} all-gather(f32[1,1,512]{2,1,0:T(1,128)S(1)} %bitcast.94), channel_id=1, replica_groups=mesh['grp'=2,'fs'=4,'tp'=4] {'fs'}, dimensions={0}, use_global_device_ids=true | all-gather | bytes 10240 | tf_op jit(solution)/shard_map/all_gather | solution.py:115
  156.2 2.6 fusion.39
  158.9 4.5 multiply_convert_fusion.8
  163.6 27.8 %all-gather.17.cloned.1.call-done = bf16[2048,512]{1,0:T(8,128)(2,1)} async-done(((bf16[512,512]{1,0:T(8,128)(2,1)}), bf16[2048,512]{1,0:T(8,128)(2,1)}) %all-gather.17.cloned.1.call-update) | async-done | bytes 2097168 | tf_op jit(solution)/shard_map/all_gather | solution.py:122
  191.4 4.5 multiply_convert_fusion.7
  197.5 74.9 %all-gather.15.cloned.1.call-done = bf16[2048,1024]{1,0:T(8,128)(2,1)} async-done(((bf16[512,1024]{1,0:T(8,128)(2,1)}), bf16[2048,1024]{1,0:T(8,128)(2,1)}) %all-gather.15.cloned.1.call-update) | async-done | bytes 4194320 | tf_op jit(solution)/shard_map/all_gather | solution.py:122
  272.4 6.9 multiply_convert_fusion.6
  279.2 2.6 reshape.110
  283.6 31.8 %while.14 = (s32[]{:T(128)}, f32[2,256,512]{2,1,0:T(8,128)S(1)}, f32[6,2,128,512]{3,2,1,0:T(8,128)}, f32[6,2,128]{2,1,0:T(2,128)S(1)}, bf16[6,2,128,256]{3,2,1,0...) while((s32[]{:T(128)}, f32[2,256,512]{2,1,0:T(8,128)S(1)}, ...), condition=%wide.region_3.4_spmd.clone.clone, body=%wide.region_1.3_spmd.clone.clone.sunk | while | flops 186269696 | bytes 5815448 | solution.py:69
  296.0 2.1 fusion.83
  301.3 2.1 fusion.83
  315.5 2.4 bitcast_reduce_fusion
  320.2 2.4 copy.49
  323.8 2.4 copy.48
  326.2 2.4 copy.41
  328.7 2.4 copy.47
  331.2 21.9 %all-gather.19.cloned.1.call-done = bf16[2048,1024]{1,0:T(8,128)(2,1)} async-done(((bf16[512,1024]{1,0:T(8,128)(2,1)}), bf16[2048,1024]{1,0:T(8,128)(2,1)}) %all-gather.19.cloned.1.call-update) | async-done | bytes 4194320 | tf_op jit(solution)/shard_map/all_gather | solution.py:122
  353.1 15.4 %fusion.49 = bf16[2048,768]{0,1:T(8,128)(2,1)} fusion(f32[2048]{0:T(1024)S(1)} %bitcast.92, bf16[1024,2048]{0,1:T(8,128)(2,1)} %bitcast.9, f32[768,1024]{1,0:T(8,128)} %bitcast.89, f32[768,1024]{1,0:T(8,128)} %bitcast.91, f32[768,1024]{1,0:T(8,128)} %bitcast.90, bf16[2048,1024]{1,0:T(8,128)(2,1)} %all-gather.19.cloned.1.call-done, f32[1024]{0:T(1024)S(1)} %copy-done.20, ...), kind=kOutput, calls=%fused_computation.63 | convolution fusion | flops 6458966016 | bytes 24140800 | tf_op jit(solution)/shard_map/dot_general | solution.py:150
  369.9 35.0 %reduce-scatter.3.cloned.1.call-done = bf16[512,768]{0,1:T(8,128)(2,1)} async-done(((bf16[2048,768]{0,1:T(8,128)(2,1)}), bf16[512,768]{0,1:T(8,128)(2,1)}) %reduce-scatter.3.cloned.1.call-update) | async-done | bytes 786448 | tf_op jit(solution)/shard_map/reduce_scatter | solution.py:148
  404.9 2.2 add_convert_fusion.1
  407.2 3.9 convert_element_type.109
  411.1 3.9 convert_element_type.111
  415.1 12.2 %all-gather.1 = f32[4,1,512]{2,1,0:T(1,128)S(1)} all-gather(f32[1,1,512]{2,1,0:T(1,128)S(1)} %bitcast.95), channel_id=1, replica_groups=mesh['grp'=2,'fs'=4,'tp'=4] {'fs'}, dimensions={0}, use_global_device_ids=true | all-gather | bytes 10240 | tf_op jit(solution)/shard_map/all_gather | solution.py:116
  427.2 8.5 %all-gather.21.cloned.1.call-done = bf16[2048,768]{0,1:T(8,128)(2,1)} async-done(((bf16[512,768]{0,1:T(8,128)(2,1)}), bf16[2048,768]{0,1:T(8,128)(2,1)}) %all-gather.21.cloned.1.call-update) | async-done | bytes 3145744 | tf_op jit(solution)/shard_map/all_gather | solution.py:33
  435.8 2.7 fusion.42
  438.5 148.5 %all-gather.23.cloned.1.call-done = bf16[2048,2048]{1,0:T(8,128)(2,1)} async-done(((bf16[512,2048]{1,0:T(8,128)(2,1)}), bf16[2048,2048]{1,0:T(8,128)(2,1)}) %all-gather.23.cloned.1.call-update) | async-done | bytes 8388624 | tf_op jit(solution)/shard_map/all_gather | solution.py:163
  587.0 149.4 %all-gather.25.cloned.1.call-done = bf16[2048,2048]{1,0:T(8,128)(2,1)} async-done(((bf16[2048,512]{1,0:T(8,128)(2,1)}), bf16[2048,2048]{1,0:T(8,128)(2,1)}) %all-gather.25.cloned.1.call-update) | async-done | bytes 8388624 | tf_op jit(solution)/shard_map/all_gather | solution.py:169
  736.4 20.6 %fusion.48 = bf16[2048,768]{0,1:T(8,128)(2,1)} fusion(f32[2048]{0:T(1024)S(1)} %bitcast.93, bf16[2048,2048]{1,0:T(8,128)(2,1)} %all-gather.25.cloned.1.call-done, bf16[2048,2048]{1,0:T(8,128)(2,1)} %all-gather.23.cloned.1.call-done, bf16[2048,768]{0,1:T(8,128)(2,1)S(1)} %copy-done.3, f32[2048]{0:T(1024)S(1)} %copy-done.17, f32[2048]{0:T(1024)S(1)} %copy-done.18, ...), kind=kOutput, calls=%fused_computation.62 | convolution fusion | flops 12900630528 | bytes 23096320 | tf_op jit(solution)/shard_map/dot_general | solution.py:168
  757.0 36.1 %reduce-scatter.5.cloned.1.call-done = bf16[512,768]{0,1:T(8,128)(2,1)} async-done(((bf16[2048,768]{0,1:T(8,128)(2,1)}), bf16[512,768]{0,1:T(8,128)(2,1)}) %reduce-scatter.5.cloned.1.call-update) | async-done | bytes 786448 | tf_op jit(solution)/shard_map/reduce_scatter | solution.py:176
  (139 shorter events, 45.1 us)
Async XLA Ops:
  6.5 3.1 copy-start.7
  6.5 4.1 copy-start.5
  6.5 149.7 %all-gather.11.cloned.1.call-start = ((), (), s32[]{:S(2)}) async-start(), calls=%async_computation.3 | async-start | bytes 3932160 | tf_op jit(solution)/shard_map/all_gather | solution.py:33
  7.3 151.6 %all-gather.13.cloned.1.call-start = ((), (), s32[]{:S(2)}) async-start(), calls=%async_computation.4 | async-start | bytes 2621440 | tf_op jit(solution)/shard_map/all_gather | solution.py:122
  9.6 181.7 %all-gather.17.cloned.1.call-start = ((), (), s32[]{:S(2)}) async-start(), calls=%async_computation.6 | async-start | bytes 2621440 | tf_op jit(solution)/shard_map/all_gather | solution.py:122
  10.6 261.8 %all-gather.15.cloned.1.call-start = ((), (), s32[]{:S(2)}) async-start(), calls=%async_computation.5 | async-start | bytes 5242880 | tf_op jit(solution)/shard_map/all_gather | solution.py:122
  16.6 6.7 copy-start.6
  16.6 314.5 %all-to-all-start = ((bf16[4,1024,512]{1,2,0:T(8,128)(2,1)}), bf16[4,1024,512]{1,2,0:T(8,128)(2,1)}, u32[]{:S(2)}, u32[]{:S(2)}) async-start(bf16[4,1024,512]{1,2,0:T(8,128)(2,1)} %stack.2), calls=%async_computation | async-start | bytes 8388608 | tf_op jit(solution)/shard_map/all_to_all | solution.py:146
  23.3 132.9 %copy-start.9 = (f32[2,768]{1,0:T(2,128)S(1)}, f32[2,768]{1,0:T(2,128)}, u32[]{:S(2)}) copy-start(f32[2,768]{1,0:T(2,128)} %param.39) | copy-start | bytes 18436
  23.3 132.9 %copy-start.14 = (f32[2]{0:T(128)S(1)}, f32[2]{0:T(128)}, u32[]{:S(2)}) copy-start(f32[2]{0:T(128)} %param.38) | copy-start | bytes 28
  23.3 135.6 %copy-start.15 = (f32[2048]{0:T(1024)S(1)}, f32[2048]{0:T(1024)}, u32[]{:S(2)}) copy-start(f32[2048]{0:T(1024)} %param.22) | copy-start | bytes 24580
  23.3 135.6 %copy-start.21 = (f32[512]{0:T(512)S(1)}, f32[512]{0:T(512)}, u32[]{:S(2)}) copy-start(f32[512]{0:T(512)} %param.27) | copy-start | bytes 6148
  23.3 329.7 %all-gather.19.cloned.1.call-start = ((), (), s32[]{:S(2)}) async-start(), calls=%async_computation.7 | async-start | bytes 5242880 | tf_op jit(solution)/shard_map/all_gather | solution.py:122
  24.5 380.4 %reduce-scatter.3.cloned.1.call-start = ((), (), s32[]{:S(2)}) async-start(), calls=%async_computation.8 | async-start | bytes 3932160 | tf_op jit(solution)/shard_map/reduce_scatter | solution.py:148
  158.8 113.5 %copy-start.10 = (f32[768]{0:T(1024)}, f32[768]{0:T(1024)S(1)}, u32[]{:S(2)}) copy-start(f32[768]{0:T(1024)S(1)} %add_rsqrt_fusion.1) | copy-start | bytes 9220
  158.8 32.5 %copy-start.22 = (f32[512]{0:T(512)S(1)}, f32[512]{0:T(512)}, u32[]{:S(2)}) copy-start(f32[512]{0:T(512)} %param.25) | copy-start | bytes 6148
  195.8 76.5 %copy-start.19 = (f32[1024]{0:T(1024)S(1)}, f32[1024]{0:T(1024)}, u32[]{:S(2)}) copy-start(f32[1024]{0:T(1024)} %param.29) | copy-start | bytes 12292
  315.4 2.9 copy-start
  328.7 24.4 %copy-start.2 = (bf16[2048,768]{1,0:T(8,128)(2,1)S(1)}, bf16[2048,768]{1,0:T(8,128)(2,1)}, u32[]{:S(2)}) copy-start(bf16[2048,768]{1,0:T(8,128)(2,1)} %all-gather.11.cloned.1.call-done) | copy-start | bytes 9437188
  328.7 24.4 %copy-start.8 = (f32[4,1,512]{2,1,0:T(1,128)S(1)}, f32[4,1,512]{2,1,0:T(1,128)}, u32[]{:S(2)}) copy-start(f32[4,1,512]{2,1,0:T(1,128)} %all-gather) | copy-start | bytes 24580
  328.7 24.4 %copy-start.11 = (f32[768]{0:T(1024)S(1)}, f32[768]{0:T(1024)}, u32[]{:S(2)}) copy-start(f32[768]{0:T(1024)} %copy-done.10) | copy-start | bytes 9220
  328.7 24.3 %copy-start.16 = (f32[2048]{0:T(1024)S(1)}, f32[2048]{0:T(1024)}, u32[]{:S(2)}) copy-start(f32[2048]{0:T(1024)} %param.22) | copy-start | bytes 24580
  328.7 24.3 %copy-start.20 = (f32[1024]{0:T(1024)S(1)}, f32[1024]{0:T(1024)}, u32[]{:S(2)}) copy-start(f32[1024]{0:T(1024)} %param.31) | copy-start | bytes 12292
  368.5 67.3 %all-gather.21.cloned.1.call-start = ((), (), s32[]{:S(2)}) async-start(), calls=%async_computation.9 | async-start | bytes 3932160 | tf_op jit(solution)/shard_map/all_gather | solution.py:33
  407.1 179.9 %all-gather.23.cloned.1.call-start = ((), (), s32[]{:S(2)}) async-start(), calls=%async_computation.10 | async-start | bytes 10485760 | tf_op jit(solution)/shard_map/all_gather | solution.py:163
  411.0 4.0 copy-start.13
  411.1 325.3 %all-gather.25.cloned.1.call-start = ((), (), s32[]{:S(2)}) async-start(), calls=%async_computation.11 | async-start | bytes 10485760 | tf_op jit(solution)/shard_map/all_gather | solution.py:169
  415.0 321.4 %copy-start.17 = (f32[2048]{0:T(1024)S(1)}, f32[2048]{0:T(1024)}, u32[]{:S(2)}) copy-start(f32[2048]{0:T(1024)} %param.35) | copy-start | bytes 24580
  415.0 321.4 %copy-start.18 = (f32[2048]{0:T(1024)S(1)}, f32[2048]{0:T(1024)}, u32[]{:S(2)}) copy-start(f32[2048]{0:T(1024)} %param.23) | copy-start | bytes 24580
  415.0 378.1 %reduce-scatter.5.cloned.1.call-start = ((), (), s32[]{:S(2)}) async-start(), calls=%async_computation.12 | async-start | bytes 3932160 | tf_op jit(solution)/shard_map/reduce_scatter | solution.py:176
  435.8 300.6 %copy-start.3 = (bf16[2048,768]{0,1:T(8,128)(2,1)S(1)}, bf16[2048,768]{0,1:T(8,128)(2,1)}, u32[]{:S(2)}) copy-start(bf16[2048,768]{0,1:T(8,128)(2,1)} %all-gather.21.cloned.1.call-done) | copy-start | bytes 9437188
  757.0 36.1 %copy-start.1 = (bf16[512,768]{0,1:T(8,128)(2,1)S(1)}, bf16[512,768]{0,1:T(8,128)(2,1)}, u32[]{:S(2)}) copy-start(bf16[512,768]{0,1:T(8,128)(2,1)} %add_convert_fusion.1) | copy-start | bytes 2359300
  (2 other events, 2.5 us)
Sparse Core Ops, SparseCore 0:
  8.9 31.2 all-gather.10
  41.7 83.7 all-gather.12
  127.1 64.1 all-gather.16
  192.8 79.5 all-gather.14
  273.8 79.2 all-gather.18
  368.6 36.1 reduce-scatter.2
  407.2 28.4 all-gather.20
  437.3 149.6 all-gather.22
  588.6 147.7 all-gather.24
  757.1 35.8 reduce-scatter.4
